TPU v7x, 32 devices: a whole 2x2x4 slice. The times are simulated.
32 devices in a mesh: grp: 2 (over y), tp: 4 (over z), dp: 4 (over x, core).
Axes of the slice: x: 2, y: 2, z: 4, core: 2. Of those that a mesh axis runs over, the one named last changes fastest.
Arguments:
- tokens: bfloat16 [64, 8, 4096], P(('grp', 'tp'), None, 'dp'), parts along dimension 0, may hold values from -6 to 6
- lengths: int32 [64], P('grp'), parts along dimension 0, may hold values from 1 to 8, 112 in all
- norm_gain: float32 [2, 4096], P(None, 'dp'), may hold values from 0.1 to 1.9
- w_recept: bfloat16 [2, 4096, 2048], P(None, 'dp', 'tp'), may hold values from -0.09375 to 0.09375
- w_key: bfloat16 [2, 4096, 2048], P(None, 'dp', 'tp'), may hold values from -0.09375 to 0.09375
- w_value: bfloat16 [2, 4096, 2048], P(None, 'dp', 'tp'), may hold values from -0.09375 to 0.09375
- w_decay: bfloat16 [2, 4096, 2048], P(None, 'dp', 'tp'), may hold values from -0.375 to 0.375
- w_rate: bfloat16 [2, 4096, 2048], P(None, 'dp', 'tp'), may hold values from -0.09375 to 0.09375
- w_gate: bfloat16 [2, 4096, 2048], P(None, 'dp', 'tp'), may hold values from -0.09375 to 0.09375
- w_out: bfloat16 [2, 2048, 4096], P(None, 'tp', 'dp'), may hold values from -0.125 to 0.125
- decay_base: float32 [2, 2048], P(None, 'tp'), may hold values from -4 to 3
- out_gain: float32 [2, 2048], P(None, 'tp'), may hold values from 0.1 to 1.9
- states: float32 [2, 64, 64, 2048], P(None, ('grp', 'dp'), None, 'tp'), parts along dimension 1, may hold values from -6 to 6
Outputs:
- stream_out: float32 [64, 8, 4096], P(('grp', 'tp'), None, 'dp'), parts along dimension 0
- new_states: float32 [2, 64, 64, 2048], P(None, ('grp', 'dp'), None, 'tp'), parts along dimension 1
There are 2 independent parts, one for each index of `grp`. A program takes and returns all parts, laid end to end along the dimension named above; an argument that names none is the same for every part. Nothing has to cross between parts.
Inputs may be any that keep to these rules, and one draw needn't show every extreme that they name: lengths[b] first tokens of sequence b are live; together they count 7 * 16 and the largest is 8.
All inputs are finite; a program needn't handle non-finite values.
Results may differ from a plain program's by a relative error of at most 0.0061.
Values may be sent and summed in bfloat16 or wider, within the bound.
A program may use at most 128 MiB of HBM per device.

v0:
```python
import jax
import jax.numpy as jnp
from jax import lax
from jax.sharding import PartitionSpec as P

D = 4096
HEAD = 64
BLOCKS = 2
group_eps = 0.00064
norm_eps = 1e-06
key_eps = 1e-06
decay_scale = 0.606531
highest = lax.Precision.HIGHEST


def mix_heads(
    state_in,
    recept,
    keys_in,
    values,
    decay_pre,
    rate_pre,
    gate_pre,
    base_shift,
    out_scale,
    live_mask,
    head_size,
):
    row_count, step_count, width_all = recept.shape
    head_count = width_all // head_size
    shape_heads = (row_count, step_count, head_count, head_size)
    decay_rate = jnp.exp(-decay_scale * jax.nn.sigmoid(decay_pre + base_shift)).reshape(shape_heads)
    learn_rate = jax.nn.sigmoid(rate_pre).reshape(shape_heads)
    key_heads = keys_in.reshape(shape_heads)
    unit_keys = key_heads * lax.rsqrt(
        jnp.sum(key_heads * key_heads, axis=3, keepdims=True) + key_eps
    )
    removal = unit_keys * learn_rate
    recept_heads = recept.reshape(shape_heads)
    value_heads = values.reshape(shape_heads)
    memory = state_in.reshape(row_count, head_size, head_count, head_size)
    outputs = []
    for position in range(step_count):
        seen_part = jnp.einsum("bihj,bhj->bhi", memory, unit_keys[:, position], precision=highest)
        updated = (
            memory * decay_rate[:, position][:, None, :, :]
            - jnp.swapaxes(seen_part, 1, 2)[:, :, :, None] * removal[:, position][:, None, :, :]
            + jnp.swapaxes(value_heads[:, position], 1, 2)[:, :, :, None]
            * key_heads[:, position][:, None, :, :]
        )
        memory = jnp.where(live_mask[:, position][:, None, None, None], updated, memory)
        outputs.append(
            jnp.einsum("bihj,bhj->bhi", memory, recept_heads[:, position], precision=highest)
        )
    readout = jnp.stack(outputs, axis=1)
    centered = readout - jnp.mean(readout, axis=3, keepdims=True)
    normed = centered * lax.rsqrt(jnp.mean(centered * centered, axis=3, keepdims=True) + group_eps)
    gated = normed.reshape(row_count, step_count, width_all) * out_scale * jax.nn.sigmoid(gate_pre)
    gated = jnp.where(live_mask[:, :, None], gated, 0.0)
    return (gated.astype(jnp.bfloat16), memory.reshape(row_count, head_size, width_all))


def body(
    tokens,
    lengths,
    norm_gain,
    w_recept,
    w_key,
    w_value,
    w_decay,
    w_rate,
    w_gate,
    w_out,
    decay_base,
    out_gain,
    states,
):
    horizon = tokens.shape[1]
    held_rows = states.shape[1]
    first_row = lax.axis_index("dp") * held_rows
    held_lengths = lax.dynamic_slice_in_dim(lengths, first_row, held_rows, 0)
    live_mask = jnp.arange(horizon, dtype=jnp.int32)[None, :] < held_lengths[:, None]
    current = tokens.astype(jnp.float32)
    finals = []
    for block_index in range(BLOCKS):
        gathered_in = lax.all_gather(current, "tp", axis=0, tiled=True)
        squares = jnp.sum(jnp.square(gathered_in), axis=2)
        total_squares = lax.psum_scatter(squares, "dp", scatter_dimension=0, tiled=True)
        inv_rms = lax.rsqrt(total_squares / D + norm_eps)
        scaled = (gathered_in * norm_gain[block_index]).astype(jnp.bfloat16)
        partials = tuple(
            (
                jnp.einsum(
                    "bsd,dc->bsc", scaled, weight[block_index], preferred_element_type=jnp.float32
                )
                for weight in (w_recept, w_key, w_value, w_decay, w_rate, w_gate)
            )
        )
        summed = lax.psum_scatter(partials, "dp", scatter_dimension=0, tiled=True)
        projected = [member * inv_rms[:, :, None] for member in summed]
        gated, final_state = mix_heads(
            states[block_index],
            projected[0],
            projected[1],
            projected[2],
            projected[3],
            projected[4],
            projected[5],
            decay_base[block_index],
            out_gain[block_index],
            live_mask,
            HEAD,
        )
        finals.append(final_state)
        all_rows = lax.all_gather(gated, "dp", axis=0, tiled=True)
        regrouped = lax.all_to_all(all_rows, "tp", split_axis=0, concat_axis=2, tiled=True)
        output = jnp.einsum(
            "bsc,cd->bsd",
            regrouped,
            lax.all_gather(w_out[block_index], "tp", axis=0, tiled=True),
            preferred_element_type=jnp.float32,
        )
        current = current + output
    return (current, jnp.stack(finals, axis=0))


def solution(mesh):
    in_specs = (
        P(("grp", "tp"), None, "dp"),
        P("grp"),
        P(None, "dp"),
        P(None, "dp", "tp"),
        P(None, "dp", "tp"),
        P(None, "dp", "tp"),
        P(None, "dp", "tp"),
        P(None, "dp", "tp"),
        P(None, "dp", "tp"),
        P(None, "tp", "dp"),
        P(None, "tp"),
        P(None, "tp"),
        P(None, ("grp", "dp"), None, "tp"),
    )
    out_specs = (P(("grp", "tp"), None, "dp"), P(None, ("grp", "dp"), None, "tp"))
    return jax.shard_map(body, mesh=mesh, in_specs=in_specs, out_specs=out_specs, check_vma=False)
```

profile of v0, /device:TPU:0, one launch (start us, length us, event | category | flops | bytes accessed | tf_op | source)
XLA Modules:
  0.0 758.3 jit_solution(8555726532389750007)
XLA Ops:
  10.4 30.4 %all-gather.7.cloned.1.call-done = f32[32,8,1024]{2,1,0:T(8,128)} async-done(((f32[8,8,1024]{2,1,0:T(8,128)}), f32[32,8,1024]{2,1,0:T(8,128)}) %all-gather.7.cloned.1.call-update) | async-done | bytes 1048592 | tf_op jit(solution)/shard_map/all_gather | solution.py:86
  64.6 10.8 %all-reduce = f32[32,8]{1,0:T(8,128)S(1)} all-reduce(f32[32,8]{1,0:T(8,128)S(1)} %get-tuple-element.12), channel_id=5, replica_groups=mesh['grp'=2,'tp'=4,'dp'=4] {'dp'}, use_global_device_ids=true, to_apply=%region_2.0.clone | all-reduce | flops 256 | bytes 2048
  75.4 13.5 %reduce-scatter.15.cloned.1.call-done = f32[8,8,512]{2,1,0:T(8,128)} async-done(((f32[32,8,512]{2,1,0:T(8,128)}), f32[8,8,512]{2,1,0:T(8,128)}) %reduce-scatter.15.cloned.1.call-update) | async-done | bytes 131088 | tf_op jit(solution)/shard_map/reduce_scatter | solution.py:99
  88.9 24.0 %reduce-scatter.17.cloned.1.call-done = f32[8,8,512]{2,1,0:T(8,128)} async-done(((f32[32,8,512]{2,1,0:T(8,128)}), f32[8,8,512]{2,1,0:T(8,128)}) %reduce-scatter.17.cloned.1.call-update) | async-done | bytes 131088 | tf_op jit(solution)/shard_map/reduce_scatter | solution.py:99
  113.0 24.0 %reduce-scatter.19.cloned.1.call-done = f32[8,8,512]{2,1,0:T(8,128)} async-done(((f32[32,8,512]{2,1,0:T(8,128)}), f32[8,8,512]{2,1,0:T(8,128)}) %reduce-scatter.19.cloned.1.call-update) | async-done | bytes 131088 | tf_op jit(solution)/shard_map/reduce_scatter | solution.py:99
  137.0 24.0 %reduce-scatter.21.cloned.1.call-done = f32[8,8,512]{2,1,0:T(8,128)} async-done(((f32[32,8,512]{2,1,0:T(8,128)}), f32[8,8,512]{2,1,0:T(8,128)}) %reduce-scatter.21.cloned.1.call-update) | async-done | bytes 131088 | tf_op jit(solution)/shard_map/reduce_scatter | solution.py:99
  190.3 5.1 add_select_fusion.13
  204.0 5.8 add_select_fusion.12
  218.4 7.1 add_select_fusion.11
  234.1 8.6 %add_select_fusion.10 = f32[8,64,8,64]{3,2,1,0:T(8,128)S(1)} fusion(f32[8,8,64]{2,1,0:T(8,128)} %get-tuple-element.52, f32[8,64,8]{2,1,0:T(8,128)} %copy.40, f32[8,8,64]{2,1,0:T(8,128)} %get-tuple-element.36, f32[8,64,8]{2,1,0:T(8,128)} %bitcast.789, f32[8,8,64]{2,1,0:T(8,128)} %get-tuple-element.20, pred[8]{0:T(512)(128)(4,1)} %get-tuple-element.176, ...), kind=kLoop, calls=%fused_computation.21 | loop fusion | flops 9437184 | bytes 2588720 | tf_op jit(solution)/shard_map/jit(_where)/select_n | solution.py:51
  251.2 10.0 %add_select_fusion.9 = f32[8,64,8,64]{3,2,1,0:T(8,128)S(1)} fusion(f32[8,8,64]{2,1,0:T(8,128)} %get-tuple-element.53, f32[8,64,8]{2,1,0:T(8,128)} %copy.41, f32[8,8,64]{2,1,0:T(8,128)} %get-tuple-element.37, f32[8,64,8]{2,1,0:T(8,128)} %bitcast.797, f32[8,8,64]{2,1,0:T(8,128)} %get-tuple-element.21, pred[8]{0:T(512)(128)(4,1)} %get-tuple-element.175, ...), kind=kLoop, calls=%fused_computation.20 | loop fusion | flops 11010048 | bytes 2670648 | tf_op jit(solution)/shard_map/jit(_where)/select_n | solution.py:51
  268.2 5.2 fusion.62
  284.1 4.8 fusion.50
  294.7 4.4 fusion.42
  304.7 10.8 %add_select_fusion.8 = f32[8,64,8,64]{3,2,1,0:T(8,128)S(1)} fusion(f32[8,8,64]{2,1,0:T(8,128)} %get-tuple-element.54, f32[8,64,8]{2,1,0:T(8,128)S(1)} %copy-done.51, f32[8,8,64]{2,1,0:T(8,128)} %get-tuple-element.38, f32[8,64,8]{2,1,0:T(8,128)S(1)} %bitcast.804, f32[8,8,64]{2,1,0:T(8,128)} %get-tuple-element.22, pred[8]{0:T(512)(128)(4,1)S(1)} %copy-done.161, ...), kind=kLoop, calls=%fused_computation.19 | loop fusion | flops 12582912 | bytes 2752576 | tf_op jit(solution)/shard_map/jit(_where)/select_n | solution.py:51
  324.7 5.8 all_gather.19
  330.4 13.7 %all_to_all.36 = bf16[32,8,512]{2,1,0:T(8,128)(2,1)S(1)} all-to-all(bf16[32,8,512]{2,1,0:T(8,128)(2,1)S(1)} %all_gather.19), channel_id=1, replica_groups=mesh['grp'=2,'tp'=4,'dp'=4] {'tp'}, dimensions={0} | all-to-all | bytes 524288 | tf_op jit(solution)/shard_map/all_to_all | solution.py:116
  348.1 26.2 %all-gather.9.cloned.1.call-done = f32[32,8,1024]{2,1,0:T(8,128)} async-done(((f32[8,8,1024]{2,1,0:T(8,128)}), f32[32,8,1024]{2,1,0:T(8,128)}) %all-gather.9.cloned.1.call-update) | async-done | bytes 1048592 | tf_op jit(solution)/shard_map/all_gather | solution.py:86
  492.1 8.9 %add_select_fusion.17 = f32[1,8,64,512]{3,2,1,0:T(8,128)} fusion(f32[1,8,64,512]{3,2,1,0:T(8,128)S(1)} %copy-done.48, f32[1,8,64,512]{3,2,1,0:T(8,128)} %mul.1722, f32[1,8,64,512]{3,2,1,0:T(8,128)} %mul.1715, f32[1,8,64,512]{3,2,1,0:T(8,128)} %mul.1711, f32[1,8,64,512]{3,2,1,0:T(8,128)} %mul.1704, f32[1,8,64,512]{3,2,1,0:T(8,128)} %mul.1700, ...), kind=kLoop, calls=%fused_computation.110 | loop fusion | flops 12582912 | bytes 19267648 | tf_op jit(solution)/shard_map/jit(_where)/select_n | solution.py:51
  501.0 10.7 %all-reduce.1 = f32[32,8]{1,0:T(8,128)S(1)} all-reduce(f32[32,8]{1,0:T(8,128)S(1)} %copy-done.146), channel_id=12, replica_groups=mesh['grp'=2,'tp'=4,'dp'=4] {'dp'}, use_global_device_ids=true, to_apply=%region_13.14.clone | all-reduce | flops 256 | bytes 2048
  526.6 5.0 fusion.32
  547.6 4.6 add_select_fusion.5
  560.8 6.2 add_select_fusion.4
  575.7 7.1 add_select_fusion.3
  591.4 8.4 %add_select_fusion.2 = f32[8,64,8,64]{3,2,1,0:T(8,128)S(1)} fusion(f32[8,8,64]{2,1,0:T(8,128)} %get-tuple-element.100, f32[8,64,8]{2,1,0:T(8,128)} %copy.49, f32[8,8,64]{2,1,0:T(8,128)} %get-tuple-element.84, f32[8,64,8]{2,1,0:T(8,128)} %bitcast.793, f32[8,8,64]{2,1,0:T(8,128)} %get-tuple-element.68, pred[8]{0:T(512)(128)(4,1)} %get-tuple-element.176, ...), kind=kLoop, calls=%fused_computation.13 | loop fusion | flops 9437184 | bytes 2588720 | tf_op jit(solution)/shard_map/jit(_where)/select_n | solution.py:51
  606.9 9.9 %add_select_fusion.1 = f32[8,64,8,64]{3,2,1,0:T(8,128)S(1)} fusion(f32[8,8,64]{2,1,0:T(8,128)} %get-tuple-element.101, f32[8,64,8]{2,1,0:T(8,128)} %copy.50, f32[8,8,64]{2,1,0:T(8,128)} %get-tuple-element.85, f32[8,64,8]{2,1,0:T(8,128)} %bitcast.800, f32[8,8,64]{2,1,0:T(8,128)} %get-tuple-element.69, pred[8]{0:T(512)(128)(4,1)} %get-tuple-element.175, ...), kind=kLoop, calls=%fused_computation.12 | loop fusion | flops 11010048 | bytes 2670648 | tf_op jit(solution)/shard_map/jit(_where)/select_n | solution.py:51
  626.0 5.2 fusion.26
  642.0 4.6 fusion.14
  652.3 10.7 %add_select_fusion = f32[8,64,8,64]{3,2,1,0:T(8,128)S(1)} fusion(f32[8,8,64]{2,1,0:T(8,128)} %get-tuple-element.102, f32[8,64,8]{2,1,0:T(8,128)} %copy.51, f32[8,8,64]{2,1,0:T(8,128)} %get-tuple-element.86, f32[8,64,8]{2,1,0:T(8,128)S(1)} %bitcast.806, f32[8,8,64]{2,1,0:T(8,128)} %get-tuple-element.70, pred[8]{0:T(512)(128)(4,1)S(1)} %copy-done.162, ...), kind=kLoop, calls=%fused_computation.11 | loop fusion | flops 12582912 | bytes 2752576 | tf_op jit(solution)/shard_map/jit(_where)/select_n | solution.py:51
  672.1 6.2 all_gather.22
  678.3 4.4 all-to-all-start.1
  737.0 8.3 %add_select_fusion.16 = f32[1,8,64,512]{3,2,1,0:T(8,128)S(1)} fusion(f32[1,8,64,512]{3,2,1,0:T(8,128)} %mul.1814, f32[1,8,64,512]{3,2,1,0:T(8,128)} %mul.1810, f32[1,8,64,512]{3,2,1,0:T(8,128)} %mul.1803, f32[1,8,64,512]{3,2,1,0:T(8,128)} %mul.1799, f32[1,8,64,512]{3,2,1,0:T(8,128)} %mul.1792, f32[1,8,64,512]{3,2,1,0:T(8,128)} %mul.1788, ...), kind=kLoop, calls=%fused_computation.109 | loop fusion | flops 12582912 | bytes 19267648 | tf_op jit(solution)/shard_map/jit(_where)/select_n | solution.py:51
  (683 shorter events, 406.8 us)
Async XLA Ops:
  7.2 35.1 %copy-start.171 = (bf16[2,1024,512]{2,1,0:T(8,128)(2,1)S(1)}, bf16[2,1024,512]{2,1,0:T(8,128)(2,1)}, u32[]{:S(2)}) copy-start(bf16[2,1024,512]{2,1,0:T(8,128)(2,1)} %param.19) | copy-start | bytes 6291460
  7.2 33.7 %all-gather.7.cloned.1.call-start = ((), (), s32[]{:S(2)}) async-start(), calls=%async_computation.14 | async-start | bytes 1310720 | tf_op jit(solution)/shard_map/all_gather | solution.py:86
  9.0 66.4 %reduce-scatter.13.cloned.1.call-start = ((), (), s32[]{:S(2)}) async-start(), calls=%async_computation.15 | async-start | bytes 655360 | tf_op jit(solution)/shard_map/reduce_scatter | solution.py:99
  43.6 45.4 %reduce-scatter.15.cloned.1.call-start = ((), (), s32[]{:S(2)}) async-start(), calls=%async_computation.16 | async-start | bytes 655360 | tf_op jit(solution)/shard_map/reduce_scatter | solution.py:99
  46.2 66.7 %reduce-scatter.17.cloned.1.call-start = ((), (), s32[]{:S(2)}) async-start(), calls=%async_computation.17 | async-start | bytes 655360 | tf_op jit(solution)/shard_map/reduce_scatter | solution.py:99
  47.6 89.4 %reduce-scatter.19.cloned.1.call-start = ((), (), s32[]{:S(2)}) async-start(), calls=%async_computation.18 | async-start | bytes 655360 | tf_op jit(solution)/shard_map/reduce_scatter | solution.py:99
  50.4 110.7 %reduce-scatter.21.cloned.1.call-start = ((), (), s32[]{:S(2)}) async-start(), calls=%async_computation.19 | async-start | bytes 655360 | tf_op jit(solution)/shard_map/reduce_scatter | solution.py:99
  51.7 271.9 %reduce-scatter.23.cloned.1.call-start = ((), (), s32[]{:S(2)}) async-start(), calls=%async_computation.20 | async-start | bytes 655360 | tf_op jit(solution)/shard_map/reduce_scatter | solution.py:99
  54.3 290.0 %all-gather.11.cloned.1.call-start = ((), (), s32[]{:S(2)}) async-start(), calls=%async_computation.28 | async-start | bytes 5242880 | tf_op jit(solution)/shard_map/all_gather | solution.py:120
  57.5 316.8 %all-gather.9.cloned.1.call-start = ((), (), s32[]{:S(2)}) async-start(), calls=%async_computation.21 | async-start | bytes 1310720 | tf_op jit(solution)/shard_map/all_gather | solution.py:86
  75.4 87.7 %copy-start.155 = (f32[8,8]{1,0:T(8,128)}, f32[8,8]{1,0:T(8,128)S(1)}, u32[]{:S(2)}) copy-start(f32[8,8]{1,0:T(8,128)S(1)} %fusion.109) | copy-start | bytes 772
  299.0 16.5 %copy-start.85 = (f32[8,8,1,64]{3,2,1,0:T(1,128)}, f32[8,8,1,64]{3,2,1,0:T(1,128)S(1)}, u32[]{:S(2)}) copy-start(f32[8,8,1,64]{3,2,1,0:T(1,128)S(1)} %fusion.42) | copy-start | bytes 49156
  322.1 22.2 %copy-start.64 = (bf16[8,8,1024]{2,1,0:T(8,128)(2,1)S(1)}, bf16[8,8,1024]{2,1,0:T(8,128)(2,1)}, u32[]{:S(2)}) copy-start(bf16[8,8,1024]{2,1,0:T(8,128)(2,1)} %param.13) | copy-start | bytes 393220
  344.3 30.0 %copy-start.160 = (f32[1,1024]{1,0:T(1,128)S(1)}, f32[1,1024]{1,0:T(1,128)}, u32[]{:S(2)}) copy-start(f32[1,1024]{1,0:T(1,128)} %get-tuple-element.158) | copy-start | bytes 12292
  348.0 163.7 %reduce-scatter.25.cloned.1.call-start = ((), (), s32[]{:S(2)}) async-start(), calls=%async_computation.22 | async-start | bytes 655360 | tf_op jit(solution)/shard_map/reduce_scatter | solution.py:99
  378.8 132.9 %reduce-scatter.27.cloned.1.call-start = ((), (), s32[]{:S(2)}) async-start(), calls=%async_computation.23 | async-start | bytes 655360 | tf_op jit(solution)/shard_map/reduce_scatter | solution.py:99
  381.4 130.4 %reduce-scatter.29.cloned.1.call-start = ((), (), s32[]{:S(2)}) async-start(), calls=%async_computation.24 | async-start | bytes 655360 | tf_op jit(solution)/shard_map/reduce_scatter | solution.py:99
  383.9 127.9 %reduce-scatter.31.cloned.1.call-start = ((), (), s32[]{:S(2)}) async-start(), calls=%async_computation.25 | async-start | bytes 655360 | tf_op jit(solution)/shard_map/reduce_scatter | solution.py:99
  386.5 125.4 %reduce-scatter.33.cloned.1.call-start = ((), (), s32[]{:S(2)}) async-start(), calls=%async_computation.26 | async-start | bytes 655360 | tf_op jit(solution)/shard_map/reduce_scatter | solution.py:99
  389.0 282.0 %reduce-scatter.35.cloned.1.call-start = ((), (), s32[]{:S(2)}) async-start(), calls=%async_computation.27 | async-start | bytes 655360 | tf_op jit(solution)/shard_map/reduce_scatter | solution.py:99
  391.6 356.2 %all-gather.13.cloned.1.call-start = ((), (), s32[]{:S(2)}) async-start(), calls=%async_computation.29 | async-start | bytes 5242880 | tf_op jit(solution)/shard_map/all_gather | solution.py:120
  475.4 12.9 %copy-start.121 = (f32[8,1,8,64]{3,2,1,0:T(8,128)S(1)}, f32[8,1,8,64]{3,2,1,0:T(8,128)}, u32[]{:S(2)}) copy-start(f32[8,1,8,64]{3,2,1,0:T(8,128)} %get-tuple-element.43) | copy-start | bytes 49156
  475.4 13.8 %copy-start.112 = (f32[8,1,8,64]{3,2,1,0:T(8,128)S(1)}, f32[8,1,8,64]{3,2,1,0:T(8,128)}, u32[]{:S(2)}) copy-start(f32[8,1,8,64]{3,2,1,0:T(8,128)} %get-tuple-element.60) | copy-start | bytes 49156
  475.4 13.9 %copy-start.120 = (f32[8,1,8,64]{3,2,1,0:T(8,128)S(1)}, f32[8,1,8,64]{3,2,1,0:T(8,128)}, u32[]{:S(2)}) copy-start(f32[8,1,8,64]{3,2,1,0:T(8,128)} %get-tuple-element.44) | copy-start | bytes 49156
  475.4 14.8 %copy-start.111 = (f32[8,1,8,64]{3,2,1,0:T(8,128)S(1)}, f32[8,1,8,64]{3,2,1,0:T(8,128)}, u32[]{:S(2)}) copy-start(f32[8,1,8,64]{3,2,1,0:T(8,128)} %get-tuple-element.61) | copy-start | bytes 49156
  475.4 14.8 %copy-start.119 = (f32[8,1,8,64]{3,2,1,0:T(8,128)S(1)}, f32[8,1,8,64]{3,2,1,0:T(8,128)}, u32[]{:S(2)}) copy-start(f32[8,1,8,64]{3,2,1,0:T(8,128)} %get-tuple-element.45) | copy-start | bytes 49156
  475.4 15.7 %copy-start.110 = (f32[8,1,8,64]{3,2,1,0:T(8,128)S(1)}, f32[8,1,8,64]{3,2,1,0:T(8,128)}, u32[]{:S(2)}) copy-start(f32[8,1,8,64]{3,2,1,0:T(8,128)} %get-tuple-element.46) | copy-start | bytes 49156
  475.4 15.8 %copy-start.118 = (f32[8,1,8,64]{3,2,1,0:T(8,128)S(1)}, f32[8,1,8,64]{3,2,1,0:T(8,128)}, u32[]{:S(2)}) copy-start(f32[8,1,8,64]{3,2,1,0:T(8,128)} %get-tuple-element.30) | copy-start | bytes 49156
  475.4 16.7 %copy-start.48 = (f32[1,8,64,512]{3,2,1,0:T(8,128)S(1)}, f32[1,8,64,512]{3,2,1,0:T(8,128)}, u32[]{:S(2)}) copy-start(f32[1,8,64,512]{3,2,1,0:T(8,128)} %mul.1726) | copy-start | bytes 3145732
  492.1 19.7 %copy-start.167 = (f32[1,512]{1,0:T(1,128)S(1)}, f32[1,512]{1,0:T(1,128)}, u32[]{:S(2)}) copy-start(f32[1,512]{1,0:T(1,128)} %get-tuple-element.167) | copy-start | bytes 6148
  646.6 16.4 %copy-start.87 = (f32[8,8,1,64]{3,2,1,0:T(1,128)}, f32[8,8,1,64]{3,2,1,0:T(1,128)S(1)}, u32[]{:S(2)}) copy-start(f32[8,8,1,64]{3,2,1,0:T(1,128)S(1)} %fusion.14) | copy-start | bytes 49156
  678.3 68.5 %all-to-all-start.1 = ((bf16[32,8,512]{2,1,0:T(8,128)(2,1)}), bf16[32,8,512]{2,1,0:T(8,128)(2,1)}, u32[]{:S(2)}, u32[]{:S(2)}) async-start(bf16[32,8,512]{2,1,0:T(8,128)(2,1)} %all_gather.22), calls=%async_computation.13 | async-start | bytes 524288 | tf_op jit(solution)/shard_map/all_to_all | solution.py:116
  (161 other events, 997.2 us)
Sparse Core Ops, SparseCore 0:
  10.1 30.6 all-gather.6
  43.7 20.9 reduce-scatter.12
  67.2 21.6 reduce-scatter.14
  91.3 21.6 reduce-scatter.16
  115.3 21.6 reduce-scatter.18
  139.3 21.6 reduce-scatter.20
  163.5 21.6 reduce-scatter.22
  186.8 80.7 all-gather.10
  348.2 26.1 all-gather.8
  379.0 20.9 reduce-scatter.24
  402.5 21.6 reduce-scatter.26
  426.5 21.6 reduce-scatter.28
  450.7 21.6 reduce-scatter.30
  474.7 21.6 reduce-scatter.32
  498.8 21.6 reduce-scatter.34
  521.9 80.7 all-gather.12
where the time goes:
time: 768 us; the launch traced here: 758 us
  local copies, waits for them, and re-layouts  245 us (32%)
  matrix products  160 us (21%)
  waiting for transfers between devices  143 us (19%)
  other arithmetic  140 us (18%)
  blocking collectives  47.2 us (6%)
  between operations  17.2 us (2%)
    select_n x18, other arithmetic, mix_heads(): jnp.where(live_mask[:, position][:, None, None, None], updated, memory)  121 us
    reduce_scatter x12, waiting for transfers between devices, body(): summed = lax.psum_scatter(partials, 'dp', scatter_dimension=0, tiled=True)  85.8 us
    mul x48, local copies, waits for them, and re-layouts, mix_heads(): jnp.swapaxes(seen_part, 1, 2)[:, :, :, None]  73.4 us
    mul x48, local copies, waits for them, and re-layouts, mix_heads(): jnp.swapaxes(value_heads[:, position], 1, 2)[:, :, :, None]  71 us
    dot_general x16, matrix products, mix_heads(): jnp.einsum('bihj,bhj->bhi', memory, recept_heads[:, position], precision=...  68.7 us
    dot_general x14, matrix products, mix_heads(): jnp.einsum('bihj,bhj->bhi', memory, unit_keys[:, position], precision=hig...  57.4 us
    all_gather x2, waiting for transfers between devices, body(): gathered_in = lax.all_gather(current, 'tp', axis=0, tiled=True)  56.7 us
    dot_general x12, matrix products, body(): jnp.einsum('bsd,dc->bsc', scaled, weight[block_index], preferred_element_...  26.4 us
  transfers between devices with their start and end apart: 17, of which 6 were waited for; matrix products, arithmetic and copies ran while one was open for 68% of the time, Pallas kernels for 0%

commit v1 on v0

--- a/solution.py
+++ b/solution.py
@@ -83,7 +83,14 @@
     current = tokens.astype(jnp.float32)
     finals = []
     for block_index in range(BLOCKS):
-        gathered_in = lax.all_gather(current, "tp", axis=0, tiled=True)
+        ring = [current]
+        for hop in range(3):
+            ring.append(lax.ppermute(ring[-1], "tp", [(dev, (dev + 1) % 4) for dev in range(4)]))
+        gathered_in = jnp.roll(
+            jnp.concatenate(ring[::-1], axis=0),
+            (lax.axis_index("tp") + 1) * ring[0].shape[0],
+            axis=0,
+        )
         squares = jnp.sum(jnp.square(gathered_in), axis=2)
         total_squares = lax.psum_scatter(squares, "dp", scatter_dimension=0, tiled=True)
         inv_rms = lax.rsqrt(total_squares / D + norm_eps)

time: 768 us -> 760 us (0.990)
  waiting for transfers between devices: 143 us -> 133 us
    all_gather x2 -> x0, waiting for transfers between devices: 56.7 us -> none  [body(): gathered_in = lax.all_gather(current, 'tp', axis=0, tiled=True)]
    ppermute x0 -> x6, waiting for transfers between devices: none -> 48.9 us  [body(): lax.ppermute(ring[-1], 'tp', [(dev, (dev + 1) % 4) for dev in range(4)])]
    unnamed x367 -> x371, local copies, waits for them, and re-layouts: 26.2 us -> 26.2 us
  transfers between devices with their start and end apart: 17 -> 21, of which waited for: 6 -> 10; matrix products, arithmetic and copies ran while one was open for 68% -> 68% of each run, Pallas kernels for 0% -> 0%
where the time goes in v1:
time: 760 us; the launch traced here: 750 us
  local copies, waits for them, and re-layouts  245 us (32%)
  matrix products  158 us (21%)
  other arithmetic  138 us (18%)
  waiting for transfers between devices  133 us (18%)
  blocking collectives  47.4 us (6%)
  between operations  19 us (2%)
  starting transfers between devices  8.41 us (1%)
    select_n x18, other arithmetic, mix_heads(): jnp.where(live_mask[:, position][:, None, None, None], updated, memory)  121 us
    reduce_scatter x12, waiting for transfers between devices, body(): summed = lax.psum_scatter(partials, 'dp', scatter_dimension=0, tiled=True)  83.7 us
    mul x48, local copies, waits for them, and re-layouts, mix_heads(): jnp.swapaxes(seen_part, 1, 2)[:, :, :, None]  73.3 us
    mul x48, local copies, waits for them, and re-layouts, mix_heads(): jnp.swapaxes(value_heads[:, position], 1, 2)[:, :, :, None]  71 us
    dot_general x16, matrix products, mix_heads(): jnp.einsum('bihj,bhj->bhi', memory, recept_heads[:, position], precision=...  68.7 us
    dot_general x14, matrix products, mix_heads(): jnp.einsum('bihj,bhj->bhi', memory, unit_keys[:, position], precision=hig...  57.4 us
    ppermute x6, waiting for transfers between devices, body(): lax.ppermute(ring[-1], 'tp', [(dev, (dev + 1) % 4) for dev in range(4)])  48.9 us
    unnamed x371, local copies, waits for them, and re-layouts  26.2 us
  transfers between devices with their start and end apart: 21, of which 10 were waited for; matrix products, arithmetic and copies ran while one was open for 68% of the time, Pallas kernels for 0%

profile of v1, /device:TPU:0, one launch (start us, length us, event | category | flops | bytes accessed | tf_op | source)
XLA Modules:
  0.0 750.0 jit_solution(12059045723461581862)
XLA Ops:
  12.2 8.3 %collective-permute-done = f32[8,8,1024]{2,1,0:T(8,128)S(1)} collective-permute-done((f32[8,8,1024]{2,1,0:T(8,128)S(1)}, f32[8,8,1024]{2,1,0:T(8,128)S(1)}, u32[]{:S(2)}, u32[]{:S(2)}) %collective-permute-start) | collective-permute-done | bytes 262176 | tf_op jit(solution)/shard_map/ppermute | solution.py:88
  20.6 9.3 %collective-permute-done.1 = f32[8,8,1024]{2,1,0:T(8,128)S(1)} collective-permute-done((f32[8,8,1024]{2,1,0:T(8,128)S(1)}, f32[8,8,1024]{2,1,0:T(8,128)S(1)}, u32[]{:S(2)}, u32[]{:S(2)}) %collective-permute-start.1) | collective-permute-done | bytes 262176 | tf_op jit(solution)/shard_map/ppermute | solution.py:88
  31.2 7.0 collective-permute-done.2
  61.5 11.2 %all-reduce = f32[32,8]{1,0:T(8,128)S(1)} all-reduce(f32[32,8]{1,0:T(8,128)S(1)} %get-tuple-element.9), channel_id=5, replica_groups=mesh['grp'=2,'tp'=4,'dp'=4] {'dp'}, use_global_device_ids=true, to_apply=%region_2.4.clone | all-reduce | flops 256 | bytes 2048
  72.7 11.3 %reduce-scatter.15.cloned.1.call-done = f32[8,8,512]{2,1,0:T(8,128)} async-done(((f32[32,8,512]{2,1,0:T(8,128)}), f32[8,8,512]{2,1,0:T(8,128)}) %reduce-scatter.15.cloned.1.call-update) | async-done | bytes 131088 | tf_op jit(solution)/shard_map/reduce_scatter | solution.py:106
  84.0 24.2 %reduce-scatter.17.cloned.1.call-done = f32[8,8,512]{2,1,0:T(8,128)} async-done(((f32[32,8,512]{2,1,0:T(8,128)}), f32[8,8,512]{2,1,0:T(8,128)}) %reduce-scatter.17.cloned.1.call-update) | async-done | bytes 131088 | tf_op jit(solution)/shard_map/reduce_scatter | solution.py:106
  108.2 24.0 %reduce-scatter.19.cloned.1.call-done = f32[8,8,512]{2,1,0:T(8,128)} async-done(((f32[32,8,512]{2,1,0:T(8,128)}), f32[8,8,512]{2,1,0:T(8,128)}) %reduce-scatter.19.cloned.1.call-update) | async-done | bytes 131088 | tf_op jit(solution)/shard_map/reduce_scatter | solution.py:106
  132.3 24.0 %reduce-scatter.21.cloned.1.call-done = f32[8,8,512]{2,1,0:T(8,128)} async-done(((f32[32,8,512]{2,1,0:T(8,128)}), f32[8,8,512]{2,1,0:T(8,128)}) %reduce-scatter.21.cloned.1.call-update) | async-done | bytes 131088 | tf_op jit(solution)/shard_map/reduce_scatter | solution.py:106
  185.5 5.1 add_select_fusion.13
  199.2 5.8 add_select_fusion.12
  213.7 7.1 add_select_fusion.11
  229.3 8.5 %add_select_fusion.10 = f32[8,64,8,64]{3,2,1,0:T(8,128)S(1)} fusion(f32[8,8,64]{2,1,0:T(8,128)} %get-tuple-element.53, f32[8,64,8]{2,1,0:T(8,128)} %copy.40, f32[8,8,64]{2,1,0:T(8,128)} %get-tuple-element.37, f32[8,64,8]{2,1,0:T(8,128)} %bitcast.789, f32[8,8,64]{2,1,0:T(8,128)} %get-tuple-element.21, pred[8]{0:T(512)(128)(4,1)} %get-tuple-element.177, ...), kind=kLoop, calls=%fused_computation.37 | loop fusion | flops 9437184 | bytes 2588720 | tf_op jit(solution)/shard_map/jit(_where)/select_n | solution.py:51
  246.4 10.0 %add_select_fusion.9 = f32[8,64,8,64]{3,2,1,0:T(8,128)S(1)} fusion(f32[8,8,64]{2,1,0:T(8,128)} %get-tuple-element.54, f32[8,64,8]{2,1,0:T(8,128)} %copy.41, f32[8,8,64]{2,1,0:T(8,128)} %get-tuple-element.38, f32[8,64,8]{2,1,0:T(8,128)} %bitcast.797, f32[8,8,64]{2,1,0:T(8,128)} %get-tuple-element.22, pred[8]{0:T(512)(128)(4,1)} %get-tuple-element.176, ...), kind=kLoop, calls=%fused_computation.36 | loop fusion | flops 11010048 | bytes 2670648 | tf_op jit(solution)/shard_map/jit(_where)/select_n | solution.py:51
  263.4 5.2 fusion.62
  279.3 4.8 fusion.50
  299.9 10.8 %add_select_fusion.8 = f32[8,64,8,64]{3,2,1,0:T(8,128)S(1)} fusion(f32[8,8,64]{2,1,0:T(8,128)} %get-tuple-element.55, f32[8,64,8]{2,1,0:T(8,128)S(1)} %copy-done.52, f32[8,8,64]{2,1,0:T(8,128)} %get-tuple-element.39, f32[8,64,8]{2,1,0:T(8,128)S(1)} %bitcast.804, f32[8,8,64]{2,1,0:T(8,128)} %get-tuple-element.23, pred[8]{0:T(512)(128)(4,1)S(1)} %copy-done.162, ...), kind=kLoop, calls=%fused_computation.35 | loop fusion | flops 12582912 | bytes 2752576 | tf_op jit(solution)/shard_map/jit(_where)/select_n | solution.py:51
  319.9 5.8 all_gather.12
  325.7 13.8 %all_to_all.36 = bf16[32,8,512]{2,1,0:T(8,128)(2,1)S(1)} all-to-all(bf16[32,8,512]{2,1,0:T(8,128)(2,1)S(1)} %all_gather.12), channel_id=1, replica_groups=mesh['grp'=2,'tp'=4,'dp'=4] {'tp'}, dimensions={0} | all-to-all | bytes 524288 | tf_op jit(solution)/shard_map/all_to_all | solution.py:123
  342.8 8.0 %collective-permute-done.3 = f32[8,8,1024]{2,1,0:T(8,128)S(1)} collective-permute-done((f32[8,8,1024]{2,1,0:T(8,128)S(1)}, f32[8,8,1024]{2,1,0:T(8,128)S(1)}, u32[]{:S(2)}, u32[]{:S(2)}) %collective-permute-start.3) | collective-permute-done | bytes 262176 | tf_op jit(solution)/shard_map/ppermute | solution.py:88
  350.8 8.2 %collective-permute-done.4 = f32[8,8,1024]{2,1,0:T(8,128)S(1)} collective-permute-done((f32[8,8,1024]{2,1,0:T(8,128)S(1)}, f32[8,8,1024]{2,1,0:T(8,128)S(1)}, u32[]{:S(2)}, u32[]{:S(2)}) %collective-permute-start.4) | collective-permute-done | bytes 262176 | tf_op jit(solution)/shard_map/ppermute | solution.py:88
  359.0 8.2 %collective-permute-done.5 = f32[8,8,1024]{2,1,0:T(8,128)S(1)} collective-permute-done((f32[8,8,1024]{2,1,0:T(8,128)S(1)}, f32[8,8,1024]{2,1,0:T(8,128)S(1)}, u32[]{:S(2)}, u32[]{:S(2)}) %collective-permute-start.5) | collective-permute-done | bytes 262176 | tf_op jit(solution)/shard_map/ppermute | solution.py:88
  483.2 8.8 %add_select_fusion.17 = f32[1,8,64,512]{3,2,1,0:T(8,128)} fusion(f32[1,8,64,512]{3,2,1,0:T(8,128)S(1)} %copy-done.48, f32[1,8,64,512]{3,2,1,0:T(8,128)} %mul.1727, f32[1,8,64,512]{3,2,1,0:T(8,128)} %mul.1720, f32[1,8,64,512]{3,2,1,0:T(8,128)} %mul.1716, f32[1,8,64,512]{3,2,1,0:T(8,128)} %mul.1709, f32[1,8,64,512]{3,2,1,0:T(8,128)} %mul.1705, ...), kind=kLoop, calls=%fused_computation.140 | loop fusion | flops 12582912 | bytes 19267648 | tf_op jit(solution)/shard_map/jit(_where)/select_n | solution.py:51
  492.0 10.4 %all-reduce.1 = f32[32,8]{1,0:T(8,128)S(1)} all-reduce(f32[32,8]{1,0:T(8,128)S(1)} %copy-done.147), channel_id=12, replica_groups=mesh['grp'=2,'tp'=4,'dp'=4] {'dp'}, use_global_device_ids=true, to_apply=%region_13.15.clone | all-reduce | flops 256 | bytes 2048
  517.5 5.0 fusion.32
  551.7 6.2 add_select_fusion.4
  566.6 7.1 add_select_fusion.3
  582.2 8.4 %add_select_fusion.2 = f32[8,64,8,64]{3,2,1,0:T(8,128)S(1)} fusion(f32[8,8,64]{2,1,0:T(8,128)} %get-tuple-element.101, f32[8,64,8]{2,1,0:T(8,128)} %copy.49, f32[8,8,64]{2,1,0:T(8,128)} %get-tuple-element.85, f32[8,64,8]{2,1,0:T(8,128)} %bitcast.793, f32[8,8,64]{2,1,0:T(8,128)} %get-tuple-element.69, pred[8]{0:T(512)(128)(4,1)} %get-tuple-element.177, ...), kind=kLoop, calls=%fused_computation.29 | loop fusion | flops 9437184 | bytes 2588720 | tf_op jit(solution)/shard_map/jit(_where)/select_n | solution.py:51
  597.7 9.9 %add_select_fusion.1 = f32[8,64,8,64]{3,2,1,0:T(8,128)S(1)} fusion(f32[8,8,64]{2,1,0:T(8,128)} %get-tuple-element.102, f32[8,64,8]{2,1,0:T(8,128)} %copy.50, f32[8,8,64]{2,1,0:T(8,128)} %get-tuple-element.86, f32[8,64,8]{2,1,0:T(8,128)} %bitcast.800, f32[8,8,64]{2,1,0:T(8,128)} %get-tuple-element.70, pred[8]{0:T(512)(128)(4,1)} %get-tuple-element.176, ...), kind=kLoop, calls=%fused_computation.28 | loop fusion | flops 11010048 | bytes 2670648 | tf_op jit(solution)/shard_map/jit(_where)/select_n | solution.py:51
  616.8 5.2 fusion.26
  643.1 10.7 %add_select_fusion = f32[8,64,8,64]{3,2,1,0:T(8,128)S(1)} fusion(f32[8,8,64]{2,1,0:T(8,128)} %get-tuple-element.103, f32[8,64,8]{2,1,0:T(8,128)} %copy.51, f32[8,8,64]{2,1,0:T(8,128)} %get-tuple-element.87, f32[8,64,8]{2,1,0:T(8,128)S(1)} %bitcast.806, f32[8,8,64]{2,1,0:T(8,128)} %get-tuple-element.71, pred[8]{0:T(512)(128)(4,1)S(1)} %copy-done.163, ...), kind=kLoop, calls=%fused_computation.27 | loop fusion | flops 12582912 | bytes 2752576 | tf_op jit(solution)/shard_map/jit(_where)/select_n | solution.py:51
  662.9 6.2 all_gather.14
  727.7 8.3 %add_select_fusion.16 = f32[1,8,64,512]{3,2,1,0:T(8,128)S(1)} fusion(f32[1,8,64,512]{3,2,1,0:T(8,128)} %mul.1819, f32[1,8,64,512]{3,2,1,0:T(8,128)} %mul.1815, f32[1,8,64,512]{3,2,1,0:T(8,128)} %mul.1808, f32[1,8,64,512]{3,2,1,0:T(8,128)} %mul.1804, f32[1,8,64,512]{3,2,1,0:T(8,128)} %mul.1797, f32[1,8,64,512]{3,2,1,0:T(8,128)} %mul.1793, ...), kind=kLoop, calls=%fused_computation.139 | loop fusion | flops 12582912 | bytes 19267648 | tf_op jit(solution)/shard_map/jit(_where)/select_n | solution.py:51
  (695 shorter events, 424.2 us)
Async XLA Ops:
  8.0 31.0 %copy-start.172 = (bf16[2,1024,512]{2,1,0:T(8,128)(2,1)S(1)}, bf16[2,1024,512]{2,1,0:T(8,128)(2,1)}, u32[]{:S(2)}) copy-start(bf16[2,1024,512]{2,1,0:T(8,128)(2,1)} %param.21) | copy-start | bytes 6291460
  8.0 64.7 %reduce-scatter.13.cloned.1.call-start = ((), (), s32[]{:S(2)}) async-start(), calls=%async_computation.14 | async-start | bytes 655360 | tf_op jit(solution)/shard_map/reduce_scatter | solution.py:106
  9.1 11.4 %collective-permute-start = (f32[8,8,1024]{2,1,0:T(8,128)S(1)}, f32[8,8,1024]{2,1,0:T(8,128)S(1)}, u32[]{:S(2)}, u32[]{:S(2)}) collective-permute-start(f32[8,8,1024]{2,1,0:T(8,128)S(1)} %convert_element_type.15), channel_id=1, source_target_pairs={{0,4},{4,8},{8,12},{12,0},{1,5},{5,9},{9,13},{13,1},{2,6},{6,10},{... | collective-permute-start | bytes 786440 | tf_op jit(solution)/shard_map/ppermute | solution.py:88
  20.6 9.3 %collective-permute-start.1 = (f32[8,8,1024]{2,1,0:T(8,128)S(1)}, f32[8,8,1024]{2,1,0:T(8,128)S(1)}, u32[]{:S(2)}, u32[]{:S(2)}) collective-permute-start(f32[8,8,1024]{2,1,0:T(8,128)S(1)} %collective-permute-done), channel_id=1, source_target_pairs={{0,4},{4,8},{8,12},{12,0},{1,5},{5,9},{9,13},{13,1},{2,6},{6,10},{... | collective-permute-start | bytes 786440 | tf_op jit(solution)/shard_map/ppermute | solution.py:88
  29.8 8.4 %collective-permute-start.2 = (f32[8,8,1024]{2,1,0:T(8,128)S(1)}, f32[8,8,1024]{2,1,0:T(8,128)S(1)}, u32[]{:S(2)}, u32[]{:S(2)}) collective-permute-start(f32[8,8,1024]{2,1,0:T(8,128)S(1)} %collective-permute-done.1), channel_id=1, source_target_pairs={{0,4},{4,8},{8,12},{12,0},{1,5},{5,9},{9,13},{13,1},{2,6},{6,10},{... | collective-permute-start | bytes 786440 | tf_op jit(solution)/shard_map/ppermute | solution.py:88
  40.3 43.7 %reduce-scatter.15.cloned.1.call-start = ((), (), s32[]{:S(2)}) async-start(), calls=%async_computation.15 | async-start | bytes 655360 | tf_op jit(solution)/shard_map/reduce_scatter | solution.py:106
  43.0 65.2 %reduce-scatter.17.cloned.1.call-start = ((), (), s32[]{:S(2)}) async-start(), calls=%async_computation.16 | async-start | bytes 655360 | tf_op jit(solution)/shard_map/reduce_scatter | solution.py:106
  44.3 87.9 %reduce-scatter.19.cloned.1.call-start = ((), (), s32[]{:S(2)}) async-start(), calls=%async_computation.17 | async-start | bytes 655360 | tf_op jit(solution)/shard_map/reduce_scatter | solution.py:106
  47.1 109.2 %reduce-scatter.21.cloned.1.call-start = ((), (), s32[]{:S(2)}) async-start(), calls=%async_computation.18 | async-start | bytes 655360 | tf_op jit(solution)/shard_map/reduce_scatter | solution.py:106
  48.5 270.4 %reduce-scatter.23.cloned.1.call-start = ((), (), s32[]{:S(2)}) async-start(), calls=%async_computation.19 | async-start | bytes 655360 | tf_op jit(solution)/shard_map/reduce_scatter | solution.py:106
  51.0 288.5 %all-gather.5.cloned.1.call-start = ((), (), s32[]{:S(2)}) async-start(), calls=%async_computation.26 | async-start | bytes 5242880 | tf_op jit(solution)/shard_map/all_gather | solution.py:127
  54.3 448.2 %reduce-scatter.25.cloned.1.call-start = ((), (), s32[]{:S(2)}) async-start(), calls=%async_computation.20 | async-start | bytes 655360 | tf_op jit(solution)/shard_map/reduce_scatter | solution.py:106
  72.7 85.6 %copy-start.156 = (f32[8,8]{1,0:T(8,128)}, f32[8,8]{1,0:T(8,128)S(1)}, u32[]{:S(2)}) copy-start(f32[8,8]{1,0:T(8,128)S(1)} %fusion.123) | copy-start | bytes 772
  294.2 16.5 %copy-start.86 = (f32[8,8,1,64]{3,2,1,0:T(1,128)}, f32[8,8,1,64]{3,2,1,0:T(1,128)S(1)}, u32[]{:S(2)}) copy-start(f32[8,8,1,64]{3,2,1,0:T(1,128)S(1)} %fusion.42) | copy-start | bytes 49156
  317.3 22.2 %copy-start.65 = (bf16[8,8,1024]{2,1,0:T(8,128)(2,1)S(1)}, bf16[8,8,1024]{2,1,0:T(8,128)(2,1)}, u32[]{:S(2)}) copy-start(bf16[8,8,1024]{2,1,0:T(8,128)(2,1)} %param.15) | copy-start | bytes 393220
  342.5 26.0 %copy-start.50 = (f32[8,8,1024]{2,1,0:T(8,128)}, f32[8,8,1024]{2,1,0:T(8,128)S(1)}, u32[]{:S(2)}) copy-start(f32[8,8,1024]{2,1,0:T(8,128)S(1)} %fusion.64) | copy-start | bytes 786436
  342.6 25.8 %copy-start.161 = (f32[1,1024]{1,0:T(1,128)S(1)}, f32[1,1024]{1,0:T(1,128)}, u32[]{:S(2)}) copy-start(f32[1,1024]{1,0:T(1,128)} %get-tuple-element.159) | copy-start | bytes 12292
  342.6 26.0 %copy-start.173 = (bf16[2,1024,512]{2,1,0:T(8,128)(2,1)S(1)}, bf16[2,1024,512]{2,1,0:T(8,128)(2,1)}, u32[]{:S(2)}) copy-start(bf16[2,1024,512]{2,1,0:T(8,128)(2,1)} %param.21) | copy-start | bytes 6291460
  342.6 8.2 %collective-permute-start.3 = (f32[8,8,1024]{2,1,0:T(8,128)S(1)}, f32[8,8,1024]{2,1,0:T(8,128)S(1)}, u32[]{:S(2)}, u32[]{:S(2)}) collective-permute-start(f32[8,8,1024]{2,1,0:T(8,128)S(1)} %fusion.64), channel_id=1, source_target_pairs={{0,4},{4,8},{8,12},{12,0},{1,5},{5,9},{9,13},{13,1},{2,6},{6,10},{... | collective-permute-start | bytes 786440 | tf_op jit(solution)/shard_map/ppermute | solution.py:88
  350.8 8.2 %collective-permute-start.4 = (f32[8,8,1024]{2,1,0:T(8,128)S(1)}, f32[8,8,1024]{2,1,0:T(8,128)S(1)}, u32[]{:S(2)}, u32[]{:S(2)}) collective-permute-start(f32[8,8,1024]{2,1,0:T(8,128)S(1)} %collective-permute-done.3), channel_id=1, source_target_pairs={{0,4},{4,8},{8,12},{12,0},{1,5},{5,9},{9,13},{13,1},{2,6},{6,10},{... | collective-permute-start | bytes 786440 | tf_op jit(solution)/shard_map/ppermute | solution.py:88
  359.0 8.2 %collective-permute-start.5 = (f32[8,8,1024]{2,1,0:T(8,128)S(1)}, f32[8,8,1024]{2,1,0:T(8,128)S(1)}, u32[]{:S(2)}, u32[]{:S(2)}) collective-permute-start(f32[8,8,1024]{2,1,0:T(8,128)S(1)} %collective-permute-done.4), channel_id=1, source_target_pairs={{0,4},{4,8},{8,12},{12,0},{1,5},{5,9},{9,13},{13,1},{2,6},{6,10},{... | collective-permute-start | bytes 786440 | tf_op jit(solution)/shard_map/ppermute | solution.py:88
  369.9 132.7 %reduce-scatter.27.cloned.1.call-start = ((), (), s32[]{:S(2)}) async-start(), calls=%async_computation.21 | async-start | bytes 655360 | tf_op jit(solution)/shard_map/reduce_scatter | solution.py:106
  372.4 130.2 %reduce-scatter.29.cloned.1.call-start = ((), (), s32[]{:S(2)}) async-start(), calls=%async_computation.22 | async-start | bytes 655360 | tf_op jit(solution)/shard_map/reduce_scatter | solution.py:106
  374.9 127.7 %reduce-scatter.31.cloned.1.call-start = ((), (), s32[]{:S(2)}) async-start(), calls=%async_computation.23 | async-start | bytes 655360 | tf_op jit(solution)/shard_map/reduce_scatter | solution.py:106
  377.5 125.1 %reduce-scatter.33.cloned.1.call-start = ((), (), s32[]{:S(2)}) async-start(), calls=%async_computation.24 | async-start | bytes 655360 | tf_op jit(solution)/shard_map/reduce_scatter | solution.py:106
  380.0 281.8 %reduce-scatter.35.cloned.1.call-start = ((), (), s32[]{:S(2)}) async-start(), calls=%async_computation.25 | async-start | bytes 655360 | tf_op jit(solution)/shard_map/reduce_scatter | solution.py:106
  382.6 356.0 %all-gather.7.cloned.1.call-start = ((), (), s32[]{:S(2)}) async-start(), calls=%async_computation.27 | async-start | bytes 5242880 | tf_op jit(solution)/shard_map/all_gather | solution.py:127
  466.5 15.8 %copy-start.119 = (f32[8,1,8,64]{3,2,1,0:T(8,128)S(1)}, f32[8,1,8,64]{3,2,1,0:T(8,128)}, u32[]{:S(2)}) copy-start(f32[8,1,8,64]{3,2,1,0:T(8,128)} %get-tuple-element.31) | copy-start | bytes 49156
  466.5 16.7 %copy-start.48 = (f32[1,8,64,512]{3,2,1,0:T(8,128)S(1)}, f32[1,8,64,512]{3,2,1,0:T(8,128)}, u32[]{:S(2)}) copy-start(f32[1,8,64,512]{3,2,1,0:T(8,128)} %mul.1731) | copy-start | bytes 3145732
  483.2 19.5 %copy-start.168 = (f32[1,512]{1,0:T(1,128)S(1)}, f32[1,512]{1,0:T(1,128)}, u32[]{:S(2)}) copy-start(f32[1,512]{1,0:T(1,128)} %get-tuple-element.168) | copy-start | bytes 6148
  637.4 16.4 %copy-start.88 = (f32[8,8,1,64]{3,2,1,0:T(1,128)}, f32[8,8,1,64]{3,2,1,0:T(1,128)S(1)}, u32[]{:S(2)}) copy-start(f32[8,8,1,64]{3,2,1,0:T(1,128)S(1)} %fusion.14) | copy-start | bytes 49156
  669.1 68.5 %all-to-all-start.1 = ((bf16[32,8,512]{2,1,0:T(8,128)(2,1)}), bf16[32,8,512]{2,1,0:T(8,128)(2,1)}, u32[]{:S(2)}, u32[]{:S(2)}) async-start(bf16[32,8,512]{2,1,0:T(8,128)(2,1)} %all_gather.14), calls=%async_computation.13 | async-start | bytes 524288 | tf_op jit(solution)/shard_map/all_to_all | solution.py:123
  (167 other events, 1083.0 us)
Sparse Core Ops, SparseCore 0:
  40.4 19.4 reduce-scatter.12
  62.4 21.6 reduce-scatter.14
  86.5 21.6 reduce-scatter.16
  110.6 21.6 reduce-scatter.18
  134.6 21.6 reduce-scatter.20
  158.6 21.6 reduce-scatter.22
  370.0 18.9 reduce-scatter.24
  391.4 21.6 reduce-scatter.26
  415.6 21.6 reduce-scatter.28
  439.6 21.6 reduce-scatter.30
  463.8 21.6 reduce-scatter.32
  487.9 21.6 reduce-scatter.34
Sparse Core Ops, SparseCore 1:
  54.4 78.3 all-gather.4
  384.7 77.8 all-gather.6
